TPU v7x, 512 devices: a 8x2x16 block of a 8x8x16 slice. The times are simulated.
512 devices in a mesh: grp: 2 (over y), sp: 32 (over z, core), tp: 8 (over x).
Axes of the slice: x: 8, y: 2, z: 16, core: 2. Of those that a mesh axis runs over, the one named last changes fastest.
The devices are a block of a 8x8x16 slice.
Arguments:
- tokens: bfloat16 [16384, 4096], P(('grp', 'sp')), parts along dimension 0, may hold values from -6 to 6
- norm_gain: bfloat16 [2, 4096], replicated, may hold values from 0.099609375 to 1.8984375
- w_query: bfloat16 [2, 4096, 2048], P(None, 'sp', 'tp'), may hold values from -0.09375 to 0.09375
- w_key: bfloat16 [2, 4096, 2048], P(None, 'sp', 'tp'), may hold values from -0.09375 to 0.09375
- w_value: bfloat16 [2, 4096, 2048], P(None, 'sp', 'tp'), may hold values from -0.09375 to 0.09375
- w_out: bfloat16 [2, 2048, 4096], P(None, 'tp', 'sp'), may hold values from -0.125 to 0.125
- offset_bias: float32 [2, 16, 15, 31], P(None, 'tp'), may hold values from -4 to 300
Outputs:
- mixed: bfloat16 [16384, 4096], P(('grp', 'sp')), parts along dimension 0
There are 2 independent parts, one for each index of `grp`. A program takes and returns all parts, laid end to end along the dimension named above; an argument that names none is the same for every part. Nothing has to cross between parts.
All inputs are finite; a program needn't handle non-finite values.
Results may differ from a plain program's by a relative error of at most 0.013.
Values may be sent and summed in bfloat16 or wider, within the bound.
A program may use at most 128 MiB of HBM per device.

v0:
```python
import jax
import jax.numpy as jnp
from jax import lax
from jax.sharding import PartitionSpec as P

HD = 128
GRID_W = 64
KR = 8
KC = 16
LAYERS = 2


norm_eps = 1e-06


def turned_gather(arrays, axis, dims):
    turned = [jnp.moveaxis(a, dim, 0) for a, dim in zip(arrays, dims)]
    both = jnp.concatenate([t.reshape(len(t), -1) for t in turned], axis=1)
    result, at, outs = (lax.all_gather(both, axis, axis=0, tiled=True), 0, [])
    for t, dim in zip(turned, dims):
        share = result[:, at : at + t[0].size].reshape(-1, *t.shape[1:])
        outs.append(jnp.moveaxis(share, 0, dim))
        at += t[0].size
    return tuple(outs)


def with_halo(block, sides, width):
    for axis, dim in sides:
        count = lax.axis_size(axis)
        forward = [(i, i + 1) for i in range(count - 1)]
        backward = [(target, source) for source, target in forward]
        low = lax.ppermute(
            lax.slice_in_dim(block, block.shape[dim] - width, None, axis=dim), axis, forward
        )
        high = lax.ppermute(lax.slice_in_dim(block, 0, width, axis=dim), axis, backward)
        block = jnp.concatenate([low, block, high], axis=dim)
    return block


def rms_rows(values, gain):
    wide = values.astype(jnp.float32)
    scaled = wide * lax.rsqrt(jnp.mean(wide * wide, axis=-1, keepdims=True) + norm_eps)
    return (scaled * gain.astype(jnp.float32)).astype(jnp.bfloat16)


def gather_rows(block_rows):
    return lax.all_gather(block_rows, "tp", axis=0, tiled=True)


def on_device(tokens, norm_gain, w_query, w_key, w_value, w_out, offset_bias):
    sp_count = lax.axis_size("sp")
    sp_index = lax.axis_index("sp")
    tp_count = lax.axis_size("tp")
    tp_index = lax.axis_index("tp")
    tok_rows = tokens.shape[0]
    local_rows = tok_rows // GRID_W
    grid_rows = local_rows * sp_count
    heads_here = offset_bias.shape[1]
    head_width = heads_here * HD
    share_rows = tok_rows // tp_count
    reach = KR // 2
    scale = HD ** (-0.5)
    columns = jnp.arange(GRID_W, dtype=jnp.int32)
    col_first = jnp.clip(columns - KC // 2, 0, GRID_W - KC)
    col_inside = (columns[None, :] >= col_first[:, None]) & (
        columns[None, :] < col_first[:, None] + KC
    )
    col_offset = jnp.clip(columns[None, :] - columns[:, None], 1 - KC, KC - 1) + KC - 1
    col_onehot = (
        jnp.arange(2 * KC - 1, dtype=jnp.int32)[:, None, None] == col_offset[None, :, :]
    ).astype(jnp.float32)
    first_row = sp_index * local_rows
    own_rows = first_row + jnp.arange(local_rows, dtype=jnp.int32)
    row_first = jnp.clip(own_rows - reach, 0, grid_rows - KR)
    band_start = row_first - first_row + reach
    row_offset = (
        row_first[:, None] + jnp.arange(KR, dtype=jnp.int32)[None, :] - own_rows[:, None] + KR - 1
    )
    row_onehot = (
        row_offset[:, :, None] == jnp.arange(2 * KR - 1, dtype=jnp.int32)[None, None, :]
    ).astype(jnp.float32)
    every_query, every_key, every_value, every_out = turned_gather(
        (w_query, w_key, w_value, w_out), "sp", (1, 1, 1, 2)
    )
    residual = tokens
    for layer_index in range(LAYERS):
        if layer_index > 0:
            normed = gather_rows(rms_rows(residual, norm_gain[layer_index]))
        else:
            normed = rms_rows(residual, norm_gain[layer_index])
        queries = jnp.dot(normed, every_query[layer_index], preferred_element_type=jnp.float32)
        keys = jnp.dot(normed, every_key[layer_index], preferred_element_type=jnp.float32)
        values = jnp.dot(normed, every_value[layer_index], preferred_element_type=jnp.float32)
        out_weight = every_out[layer_index]
        queries = queries.astype(jnp.bfloat16).reshape(local_rows, GRID_W, heads_here, HD)
        key_values = jnp.concatenate(
            [keys.astype(jnp.bfloat16), values.astype(jnp.bfloat16)], axis=1
        )
        key_values = key_values.reshape(local_rows, GRID_W, 2 * head_width)
        padded = with_halo(key_values, (("sp", 0),), reach)
        bands = jax.vmap(lambda band_begin: lax.dynamic_slice_in_dim(padded, band_begin, KR, 0))(
            band_start
        )
        band_keys = bands[..., :head_width].reshape(local_rows, KR, GRID_W, heads_here, HD)
        band_values = bands[..., head_width:].reshape(local_rows, KR, GRID_W, heads_here, HD)
        col_bias = jnp.einsum(
            "hro,oqk->hrqk", offset_bias[layer_index], col_onehot, precision=lax.Precision.HIGHEST
        )
        full_bias = jnp.einsum(
            "ijr,hrqk->hiqjk", row_onehot, col_bias, precision=lax.Precision.HIGHEST
        )
        scores = jnp.einsum(
            "iqhd,ijkhd->hiqjk", queries, band_keys, preferred_element_type=jnp.float32
        )
        scores = scores * scale + full_bias
        scores = jnp.where(col_inside[None, None, :, None, :], scores, -jnp.inf)
        flattened = scores.reshape(heads_here, local_rows, GRID_W, KR * GRID_W)
        weights = jax.nn.softmax(flattened, axis=-1).astype(jnp.bfloat16)
        weights = weights.reshape(heads_here, local_rows, GRID_W, KR, GRID_W)
        attended = jnp.einsum(
            "hiqjk,ijkhd->iqhd", weights, band_values, preferred_element_type=jnp.float32
        )
        attended = attended.astype(jnp.bfloat16).reshape(tok_rows, head_width)

        def term_rows(row_begin, row_count, attended=attended, out_weight=out_weight):
            return jnp.dot(attended, out_weight, preferred_element_type=jnp.float32)

        branch = lax.psum_scatter(
            term_rows(jnp.int32(0), lax.axis_size("tp") * share_rows).astype(jnp.bfloat16),
            "tp",
            scatter_dimension=0,
            tiled=True,
        ).astype(jnp.float32)
        if layer_index > 0:
            own_part = residual
        else:
            own_part = lax.dynamic_slice_in_dim(tokens, tp_index * share_rows, share_rows, 0)
        residual = (own_part.astype(jnp.float32) + branch).astype(jnp.bfloat16)
    residual = gather_rows(residual)
    return residual


def solution(mesh):
    return jax.shard_map(
        on_device,
        mesh=mesh,
        in_specs=(
            P(("grp", "sp"), None),
            P(),
            P(None, "sp", "tp"),
            P(None, "sp", "tp"),
            P(None, "sp", "tp"),
            P(None, "tp", "sp"),
            P(None, "tp", None, None),
        ),
        out_specs=P(("grp", "sp"), None),
        check_vma=False,
    )
```

profile of v0, /device:TPU:80, one launch (start us, length us, event | category | flops | bytes accessed | tf_op | source)
XLA Modules:
  0.0 438.5 jit_solution(5943801142886471088)
XLA Ops:
  9.7 1.7 pad_maximum_fusion.2
  12.5 2.4 fusion.52
  14.9 2.3 copy.26
  17.8 2.1 fusion
  20.6 154.9 %all-gather.4.cloned.1.call-done = bf16[4096,2048]{0,1:T(8,128)(2,1)} async-done(((bf16[128,2048]{0,1:T(8,128)(2,1)}), bf16[4096,2048]{0,1:T(8,128)(2,1)}) %all-gather.4.cloned.1.call-update) | async-done | bytes 16777232 | tf_op jit(solution)/shard_map/all_gather | solution.py:19
  175.5 10.2 %fusion.60 = (bf16[4096,512]{0,1:T(8,128)(2,1)}, bf16[4096,512]{0,1:T(8,128)(2,1)}, bf16[4096,512]{0,1:T(8,128)(2,1)S(1)}, bf16[4096,512]{0,1:T(8,128)(2,1)S(1)}) fusion(bf16[4096,2048]{0,1:T(8,128)(2,1)} %all-gather.4.cloned.1.call-done), kind=kLoop, calls=%fused_computation.110 | loop fusion | bytes 33554432 | tf_op jit(solution)/shard_map/slice | solution.py:21
  189.1 2.2 collective-permute-start
  192.6 3.0 fusion.17
  197.5 2.1 gather_fusion
  199.6 1.9 slice_bitcast_fusion.30
  204.7 2.0 convolution_convert_fusion.1
  206.9 49.0 %reduce-scatter.3.cloned.1.call-done = bf16[32,4096]{1,0:T(8,128)(2,1)} async-done(((bf16[256,4096]{1,0:T(8,128)(2,1)}), bf16[32,4096]{1,0:T(8,128)(2,1)}) %reduce-scatter.3.cloned.1.call-update) | async-done | bytes 262160 | tf_op jit(solution)/shard_map/reduce_scatter | solution.py:128
  259.0 2.4 fusion.50
  261.3 2.3 copy.33
  263.6 41.2 %all-gather.6.cloned.1.call-done = bf16[256,4096]{1,0:T(8,128)(2,1)} async-done(((bf16[32,4096]{1,0:T(8,128)(2,1)}), bf16[256,4096]{1,0:T(8,128)(2,1)}) %all-gather.6.cloned.1.call-update) | async-done | bytes 2097168 | tf_op jit(solution)/shard_map/all_gather | solution.py:47
  304.9 3.1 fusion.18
  308.3 2.3 fusion.19
  313.5 3.0 fusion.20
  318.8 2.0 gather_fusion.1
  320.8 1.9 slice_bitcast_fusion.28
  325.9 2.0 convolution_convert_fusion
  328.1 52.2 %reduce-scatter.5.cloned.1.call-done = bf16[32,4096]{1,0:T(8,128)(2,1)} async-done(((bf16[256,4096]{1,0:T(8,128)(2,1)}), bf16[32,4096]{1,0:T(8,128)(2,1)}) %reduce-scatter.5.cloned.1.call-update) | async-done | bytes 262160 | tf_op jit(solution)/shard_map/reduce_scatter | solution.py:128
  382.0 46.8 %all-gather.8.cloned.1.call-done = bf16[256,4096]{1,0:T(8,128)(2,1)} async-done(((bf16[32,4096]{1,0:T(8,128)(2,1)}), bf16[256,4096]{1,0:T(8,128)(2,1)}) %all-gather.8.cloned.1.call-update) | async-done | bytes 2097168 | tf_op jit(solution)/shard_map/all_gather | solution.py:47
  428.9 3.1 copy.111
  (84 shorter events, 28.7 us)
Async XLA Ops:
  6.5 5.0 %copy-start.12 = (f32[2,2,15,31]{3,1,2,0:T(2,128)S(1)}, f32[2,2,15,31]{3,1,2,0:T(2,128)}, u32[]{:S(2)}) copy-start(f32[2,2,15,31]{3,1,2,0:T(2,128)} %param.13) | copy-start | bytes 22324
  6.5 168.9 %all-gather.4.cloned.1.call-start = ((), (), s32[]{:S(2)}) async-start(), calls=%async_computation.2 | async-start | bytes 17301504 | tf_op jit(solution)/shard_map/all_gather | solution.py:19
  11.5 244.4 %reduce-scatter.3.cloned.1.call-start = ((), (), s32[]{:S(2)}) async-start(), calls=%async_computation.3 | async-start | bytes 2359296 | tf_op jit(solution)/shard_map/reduce_scatter | solution.py:128
  12.5 2.4 copy-start.13
  17.2 2.7 copy-start.9
  175.5 10.2 %copy-start.5 = (bf16[256,4096]{1,0:T(8,128)(2,1)S(1)}, bf16[256,4096]{1,0:T(8,128)(2,1)}, u32[]{:S(2)}) copy-start(bf16[256,4096]{1,0:T(8,128)(2,1)} %param.7) | copy-start | bytes 6291460
  185.7 1.9 copy-start.2
  185.7 3.2 copy-start.4
  189.1 6.6 %collective-permute-start = (bf16[4,64,512]{2,1,0:T(8,128)(2,1)S(1)}, bf16[4,64,512]{2,1,0:T(8,128)(2,1)S(1)}, u32[]{:S(2)}, u32[]{:S(2)}) collective-permute-start(bf16[4,64,512]{2,1,0:T(8,128)(2,1)S(1)} %bitcast.167), channel_id=1, source_target_pairs={{0,8},{8,16},{16,24},{24,32},{32,40},{40,48},{48,56},{56,64},{64,7... | collective-permute-start | bytes 786440 | tf_op jit(solution)/shard_map/ppermute | solution.py:32
  191.3 5.1 %collective-permute-start.1 = (bf16[4,64,512]{2,1,0:T(8,128)(2,1)S(1)}, bf16[4,64,512]{2,1,0:T(8,128)(2,1)}, u32[]{:S(2)}, u32[]{:S(2)}) collective-permute-start(bf16[4,64,512]{2,1,0:T(8,128)(2,1)S(1)} %bitcast.168), channel_id=1, source_target_pairs={{8,0},{16,8},{24,16},{32,24},{40,32},{48,40},{56,48},{64,56},{72,6... | collective-permute-start | bytes 786440 | tf_op jit(solution)/shard_map/ppermute | solution.py:35
  195.7 0.7 copy-start.7
  202.5 2.2 copy-start
  206.7 50.4 %copy-start.10 = (f32[1,4096]{1,0:T(1,128)S(1)}, f32[1,4096]{1,0:T(1,128)}, u32[]{:S(2)}) copy-start(f32[1,4096]{1,0:T(1,128)} %get-tuple-element.17) | copy-start | bytes 49156
  206.7 52.2 %copy-start.14 = (s32[4,8]{1,0:T(4,128)S(1)}, s32[4,8]{1,0:T(4,128)}, u32[]{:S(2)}) copy-start(s32[4,8]{1,0:T(4,128)} %copy-done.13) | copy-start | bytes 388
  206.8 98.1 %all-gather.6.cloned.1.call-start = ((), (), s32[]{:S(2)}) async-start(), calls=%async_computation.4 | async-start | bytes 2359296 | tf_op jit(solution)/shard_map/all_gather | solution.py:47
  258.0 122.3 %reduce-scatter.5.cloned.1.call-start = ((), (), s32[]{:S(2)}) async-start(), calls=%async_computation.5 | async-start | bytes 2359296 | tf_op jit(solution)/shard_map/reduce_scatter | solution.py:128
  304.9 3.4 copy-start.3
  310.8 5.6 %copy-start.6 = (bf16[256,512]{1,0:T(8,128)(2,1)}, bf16[256,512]{1,0:T(8,128)(2,1)S(1)}, u32[]{:S(2)}) copy-start(bf16[256,512]{1,0:T(8,128)(2,1)S(1)} %copy.30) | copy-start | bytes 786436
  310.8 8.0 %copy-start.11 = (s32[4]{0:T(128)S(1)}, s32[4]{0:T(128)}, u32[]{:S(2)}) copy-start(s32[4]{0:T(128)} %shift-left_bitcast_fusion) | copy-start | bytes 52
  310.8 5.7 %collective-permute-start.2 = (bf16[4,64,512]{2,1,0:T(8,128)(2,1)S(1)}, bf16[4,64,512]{2,1,0:T(8,128)(2,1)S(1)}, u32[]{:S(2)}, u32[]{:S(2)}) collective-permute-start(bf16[4,64,512]{2,1,0:T(8,128)(2,1)S(1)} %bitcast.170), channel_id=1, source_target_pairs={{0,8},{8,16},{16,24},{24,32},{32,40},{40,48},{48,56},{56,64},{64,7... | collective-permute-start | bytes 786440 | tf_op jit(solution)/shard_map/ppermute | solution.py:32
  312.2 5.5 %collective-permute-start.3 = (bf16[4,64,512]{2,1,0:T(8,128)(2,1)S(1)}, bf16[4,64,512]{2,1,0:T(8,128)(2,1)}, u32[]{:S(2)}, u32[]{:S(2)}) collective-permute-start(bf16[4,64,512]{2,1,0:T(8,128)(2,1)S(1)} %bitcast.171), channel_id=1, source_target_pairs={{8,0},{16,8},{24,16},{32,24},{40,32},{48,40},{56,48},{64,56},{72,6... | collective-permute-start | bytes 786440 | tf_op jit(solution)/shard_map/ppermute | solution.py:35
  316.5 0.7 copy-start.8
  323.7 2.2 copy-start.1
  328.0 100.9 %all-gather.8.cloned.1.call-start = ((), (), s32[]{:S(2)}) async-start(), calls=%async_computation.6 | async-start | bytes 2359296 | tf_op jit(solution)/shard_map/all_gather | solution.py:47
Sparse Core Ops, SparseCore 0:
  11.6 163.8 all-gather.3
  206.9 48.9 reduce-scatter.2
  258.1 46.6 all-gather.5
  328.1 52.0 reduce-scatter.4
  382.2 46.6 all-gather.7
where the time goes:
time: 440 us; the launch traced here: 439 us
  waiting for transfers between devices  345 us (78%)
  local copies, waits for them, and re-layouts  35.7 us (8%)
  matrix products  25.7 us (6%)
  between operations  13.6 us (3%)
  other arithmetic  12.2 us (3%)
  starting transfers between devices  6.58 us (1%)
    all_gather x1, waiting for transfers between devices, turned_gather(): result, at, outs = (lax.all_gather(both, axis, axis=0, tiled=True), 0, [])  155 us
    reduce_scatter x2, waiting for transfers between devices, on_device(): lax.psum_scatter(term_rows(jnp.int32(0), lax.axis_size('tp') * share_rows...  101 us
    all_gather x2, waiting for transfers between devices, gather_rows(): return lax.all_gather(block_rows, 'tp', axis=0, tiled=True)  88 us
    unnamed x36, local copies, waits for them, and re-layouts  16.1 us
    slice x1, local copies, waits for them, and re-layouts, turned_gather(): share = result[:, at:at + t[0].size].reshape(-1, *t.shape[1:])  10.2 us
  transfers between devices with their start and end apart: 9, of which 6 were waited for; matrix products, arithmetic and copies ran while one was open for 5% of the time, Pallas kernels for 0%

commit v1 on v0

v1 whole, which is shorter than its diff:
```python
import functools

import jax
import jax.numpy as jnp
from jax import lax
from jax.experimental import pallas as pl
from jax.experimental.pallas import tpu as pltpu
from jax.sharding import PartitionSpec as P

HD = 128
GRID_W = 64
KR = 8
KC = 16
LAYERS = 2
LANES = 128
MESH = pl.DeviceIdType.MESH
F32 = jnp.float32
BF16 = jnp.bfloat16

norm_eps = 1e-06


def reach(n, parity):
    plus = n // 2 if parity == 0 else n // 2 - 1
    return plus, n - 1 - plus


def nt_dot(a, b):
    return lax.dot_general(a, b, (((1,), (1,)), ((), ())), preferred_element_type=F32)


def wait_bytes(ref, sem):
    pltpu.make_async_copy(ref, ref, sem).wait()


def send(src, dst, send_sem, recv_sem, device):
    pltpu.make_async_remote_copy(
        src_ref=src,
        dst_ref=dst,
        send_sem=send_sem,
        recv_sem=recv_sem,
        device_id=device,
        device_id_type=MESH,
    ).start()


def layers_kernel(
    nsp,
    nx,
    tok,
    gain0,
    gain1,
    wq,
    wk,
    wv,
    wout,
    bias,
    out,
    w0,
    w1,
    wo,
    wt,
    xn,
    acc,
    res,
    qbuf,
    kv,
    att,
    xbuf,
    ybuf,
    ss,
    ring_recv,
    part_recv,
    halo_recv,
    att_recv,
    x_recv,
    a2a_recv,
    z_send,
    part_send,
    halo_send,
    att_send,
    x_send,
    a2a_send,
    out_sem,
):
    nz = nsp // 2
    hz, hx = nz // 2, nx // 2
    me_s, me_x = lax.axis_index("sp"), lax.axis_index("tp")
    me_z, me_c = me_s // 2, me_s % 2
    toks, depth = tok.shape
    part = LANES // nx
    wide = 2 * HD
    piece_w = depth // nx
    rows = toks // GRID_W
    half = toks // 2

    def ring_s(step):
        return lax.rem(me_s + 2 * step + 2 * nsp, nsp)

    def ring_x(step):
        return lax.rem(me_x + step + nx, nx)

    z_dev = ({"sp": ring_s(1)}, {"sp": ring_s(-1)})
    x_dev = ({"tp": ring_x(1)}, {"tp": ring_x(-1)})
    partner = {"sp": me_s + 1 - 2 * me_c}
    halo_dev = (
        {"sp": lax.rem(me_s + nsp - 1, nsp)},
        {"sp": lax.rem(me_s + 1, nsp)},
    )

    barrier = pltpu.get_barrier_semaphore()
    peers = [*z_dev, *halo_dev] + [{"tp": ring_x(d)} for d in range(1, nx)]
    for peer in peers:
        pl.semaphore_signal(barrier, inc=1, device_id=peer, device_id_type=MESH)
    pl.semaphore_wait(barrier, len(peers))

    mats = (wk, wv, wq)
    kinds = (0, 1, 2)
    OUT = 3
    parity = (0, 1, 0, 1)

    def chunk(layer, kind, s):
        if kind == OUT:
            return wo.at[layer, s]
        return w0.at[kind, s] if layer == 0 else w1.at[kind, :, s]

    def part_sem(layer, kind, hop):
        if kind == OUT:
            return part_recv.at[hz + 1 + layer]
        return part_recv.at[hop] if layer == 0 else part_recv.at[hz + 3]

    def ring_slot(layer, kind, side, hop):
        return ring_recv.at[layer, kind, side * hz + hop - 1]

    def ring_start(layer, kind):
        dst = chunk(layer, kind, me_s)
        src = dst if kind == OUT else mats[kind].at[layer]
        for side in (0, 1):
            if reach(nz, parity[kind])[side] >= 1:
                send(src, dst, z_send.at[side], ring_slot(layer, kind, side, 1), z_dev[side])
        send(src, dst, part_send.at[layer], part_sem(layer, kind, 0), partner)

    def ring_hop(layer, kind, hop):
        for side in (0, 1):
            last = reach(nz, parity[kind])[side]
            if isinstance(hop, int) and hop > last:
                continue
            src = chunk(layer, kind, ring_s(-hop if side == 0 else hop))
            wait_bytes(src, ring_slot(layer, kind, side, hop))

            def onward(src=src, side=side):
                send(src, src, z_send.at[side], ring_slot(layer, kind, side, hop + 1), z_dev[side])

            if isinstance(hop, int):
                if hop < last:
                    onward()
            else:
                pl.when(hop < last)(onward)
            send(src, src, part_send.at[layer], part_sem(layer, kind, hop), partner)

    pending = []

    def service(count):
        for _ in range(min(count, len(pending))):
            ring_hop(*pending.pop(0))

    for kind in kinds:
        ring_start(0, kind)

    eye = (
        lax.broadcasted_iota(jnp.int32, (LANES, LANES), 0)
        == lax.broadcasted_iota(jnp.int32, (LANES, LANES), 1)
    ).astype(BF16)
    for layer in range(LAYERS):
        turned = nt_dot(eye, wout[layer]).astype(BF16)
        wt[layer] = turned.reshape(nx, part, wide)
    own_lanes = pl.ds(pl.multiple_of(me_x * wide, wide), wide)
    for layer in range(LAYERS):
        for d in range(1, nx):
            to = ring_x(d)
            send(
                wt.at[layer, to],
                wo.at[layer, me_s, :, own_lanes],
                a2a_send,
                a2a_recv.at[layer],
                {"tp": to},
            )
        wo[layer, me_s, :, own_lanes] = wt[layer, me_x]
    for kind in kinds:
        w0[kind, me_s] = mats[kind][0]
        w1[kind, :, me_s] = mats[kind][1]

    block = 32

    def norm_rows(i, carry):
        at = pl.ds(pl.multiple_of(i * block, block), block)
        x = tok[at, :].astype(F32)
        scaled = x * lax.rsqrt(jnp.mean(x * x, axis=-1, keepdims=True) + norm_eps)
        xn[at, :] = (scaled * gain0[...].astype(F32)).astype(BF16)
        return carry

    lax.fori_loop(0, toks // block, norm_rows, 0)

    wait_bytes(wt.at[0, pl.ds(0, nx - 1)], a2a_recv.at[0])
    ring_start(0, OUT)

    def qkv_block(z, kind):
        x = xn[:, pl.ds(pl.multiple_of(z * 2 * LANES, 2 * LANES), 2 * LANES)]
        w = w0[kind, pl.ds(2 * z, 2)].reshape(2 * LANES, wide)
        return jnp.dot(x, w, preferred_element_type=F32)

    wait_bytes(w0.at[0, pl.ds(0, 3)], part_recv.at[0])
    for kind in kinds:
        acc[:, kind * wide : (kind + 1) * wide] = qkv_block(me_z, kind)

    def two_sides(hop):
        wait_bytes(w0.at[:, pl.ds(0, 2)], part_recv.at[hop])
        before = lax.rem(me_z - hop + nz, nz)
        after = lax.rem(me_z + hop, nz)
        for kind in kinds:
            acc[:, kind * wide : (kind + 1) * wide] += qkv_block(before, kind) + qkv_block(
                after, kind
            )

    def ring_step(hop, carry):
        for kind in (*kinds, OUT):
            ring_hop(0, kind, hop)

        @pl.when(hop > 1)
        def _():
            two_sides(hop - 1)

        return carry

    lax.fori_loop(1, hz, ring_step, 0)

    group = nx * LANES
    sel_row = lax.broadcasted_iota(jnp.int32, (group, LANES), 0)
    sel_col = lax.broadcasted_iota(jnp.int32, (group, LANES), 1)
    pick = (sel_col // part) * LANES + me_x * part + sel_col % part
    sel = (sel_row == pick).astype(BF16)
    for g in range(depth // group):
        picked = jnp.dot(tok[:, g * group : (g + 1) * group], sel, preferred_element_type=F32)
        res[:, g * LANES : (g + 1) * LANES] = picked.astype(BF16)

    for kind in kinds:
        ring_hop(0, kind, hz)
    if hz > 1:
        two_sides(hz - 1)
    for kind in kinds:
        ring_start(1, kind)
    wait_bytes(w0.at[0, pl.ds(0, 3)], part_recv.at[hz])
    far = lax.rem(me_z + hz, nz)

    def store_kind(layer, kind, value):
        if kind == 2:
            qbuf[...] = value.astype(BF16)
            return
        kv[layer, kind, toks : 2 * toks] = value.astype(BF16)
        src = kv.at[layer, kind, pl.ds(toks, toks)]
        for side in (0, 1):
            dst = kv.at[layer, kind, pl.ds(2 * toks if side == 0 else 0, toks)]
            send(src, dst, halo_send.at[layer], halo_recv.at[layer, kind, side], halo_dev[side])

    for kind in kinds:
        store_kind(0, kind, acc[:, kind * wide : (kind + 1) * wide] + qkv_block(far, kind))
    ring_hop(0, OUT, hz)
    pending += [(1, kind, hop) for hop in range(1, hz + 1) for kind in kinds]

    q_col = lax.broadcasted_iota(jnp.int32, (GRID_W, KR * GRID_W), 0)
    k_col = lax.broadcasted_iota(jnp.int32, (GRID_W, KR * GRID_W), 1) % GRID_W
    first_col = jnp.clip(q_col - KC // 2, 0, GRID_W - KC)
    inside = (k_col >= first_col) & (k_col < first_col + KC)
    grid_rows = rows * nsp

    def attend(layer, i, head):
        row = me_s * rows + i
        start = jnp.clip(row - KR // 2, 0, grid_rows - KR) - (me_s * rows - rows)
        keys_at = pl.ds(pl.multiple_of(start * GRID_W, GRID_W), KR * GRID_W)
        lanes = slice(head * HD, (head + 1) * HD)
        q = qbuf[i * GRID_W : (i + 1) * GRID_W, lanes]
        scores = nt_dot(q, kv[layer, 0, keys_at, lanes]) * (HD**-0.5)
        offset = start - rows - i + KR - 1
        pairs = []
        for p in range(KR // 2):
            line = bias[layer, head, pl.ds(offset + 2 * p, 1), :]
            spread = jnp.broadcast_to(line, (GRID_W, LANES))
            pairs.append(pltpu.roll(spread, 0, 1, stride=1, stride_axis=0))
        scores = scores + jnp.concatenate(pairs, axis=1)
        scores = jnp.where(inside, scores, -jnp.inf)
        e = jnp.exp(scores - jnp.max(scores, axis=-1, keepdims=True))
        weights = (e / jnp.sum(e, axis=-1, keepdims=True)).astype(BF16)
        values = kv[layer, 1, keys_at, lanes]
        mixed = jnp.dot(weights, values, preferred_element_type=F32)
        att[layer, me_x, i, :, lanes] = mixed.astype(BF16)

    def att_hop(layer, i, hop):
        for side in (0, 1):
            last = reach(nx, i % 2)[side]
            if hop > last:
                continue
            src = att.at[layer, ring_x(-hop if side == 0 else hop), i]
            if hop > 0:
                wait_bytes(src, att_recv.at[layer, i, side * hx + hop - 1])
            if hop < last:
                slot = att_recv.at[layer, i, side * hx + hop]
                send(src, src, att_send.at[layer, side], slot, x_dev[side])

    def attention(layer):
        for kind in (0, 1):
            for side in (0, 1):
                dst = kv.at[layer, kind, pl.ds(2 * toks if side == 0 else 0, toks)]
                wait_bytes(dst, halo_recv.at[layer, kind, side])
        for i in range(rows):
            for head in (0, 1):
                attend(layer, i, head)
            att_hop(layer, i, 0)
            if layer == 0:
                service(1)
        for hop in range(1, hx + 1):
            for i in range(rows):
                att_hop(layer, i, hop)
            if layer == 0:
                service(2)

    def x_hop(layer, h, hop):
        buf = xbuf if layer == 0 else ybuf
        for side in (0, 1):
            last = reach(nx, h)[side]
            if hop > last:
                continue
            owner = ring_x(-hop if side == 0 else hop)
            src = buf.at[owner, h]
            if hop > 0:
                wait_bytes(src, x_recv.at[layer, h, side * hx + hop - 1])
            if hop < last:
                slot = x_recv.at[layer, h, side * hx + hop]
                send(src, src, x_send.at[layer, side], slot, x_dev[side])
            if layer == 1 and (hop > 0 or side == 0):
                pltpu.make_async_copy(src, out.at[owner, h], out_sem).start()

    def project(layer):
        wait_bytes(wo.at[layer, pl.ds(0, nz)], part_recv.at[hz + 1 + layer])
        buf = xbuf if layer == 0 else ybuf
        for h in (0, 1):
            total = None
            for x in range(nx):
                a = att[layer, x, h * (rows // 2) : (h + 1) * (rows // 2)].reshape(half, wide)
                w = wo[layer, :, :, x * wide : (x + 1) * wide].reshape(piece_w, wide)
                term = nt_dot(a, w)
                total = term if total is None else total + term
            own = res[h * half : (h + 1) * half] if layer == 0 else xbuf[me_x, h]
            buf[me_x, h] = (own.astype(F32) + total).astype(BF16)
            x_hop(layer, h, 0)

    attention(0)
    project(0)

    acc[...] = jnp.zeros_like(acc)
    ss[...] = jnp.zeros_like(ss)

    def qkv_piece(owner, h):
        at = slice(h * half, (h + 1) * half)
        x = xbuf[owner, h].astype(F32)
        squares = x * x
        partial = ss[at]
        for g in range(piece_w // LANES):
            partial = partial + squares[:, g * LANES : (g + 1) * LANES]
        ss[at] = partial
        xg = (x * gain1[owner]).astype(BF16)
        for kind in kinds:
            w = w1[kind, owner].reshape(piece_w, wide)
            lanes = slice(kind * wide, (kind + 1) * wide)
            acc[at, lanes] += jnp.dot(xg, w, preferred_element_type=F32)

    def owners(hop):
        if hop == 0 or hop == hx:
            return [ring_x(hop)]
        return [ring_x(-hop), ring_x(hop)]

    early = hx // 2
    share = -(-len(pending) // max(2 * early, 1))
    for hop in range(1, early + 1):
        for h in (0, 1):
            x_hop(0, h, hop)
            service(share)
    service(len(pending))
    wait_bytes(wt.at[1, pl.ds(0, nx - 1)], a2a_recv.at[1])
    ring_start(1, OUT)
    pending += [(1, OUT, hop) for hop in range(1, hz + 1)]
    wait_bytes(w0.at[:, pl.ds(0, nz)], part_recv.at[hz + 3])
    for hop in range(0, early + 1):
        for owner in owners(hop):
            for h in (0, 1):
                qkv_piece(owner, h)
        service(1)
    for hop in range(early + 1, hx + 1):
        for h in (0, 1):
            x_hop(0, h, hop)
        service(1)
        for owner in owners(hop):
            for h in (0, 1):
                qkv_piece(owner, h)
    mean = jnp.sum(ss[...], axis=-1, keepdims=True) * (1.0 / depth)
    scale = lax.rsqrt(mean + norm_eps)
    for kind in kinds:
        store_kind(1, kind, acc[:, kind * wide : (kind + 1) * wide] * scale)
    service(len(pending))
    attention(1)
    project(1)
    for hop in range(1, hx + 1):
        for h in (0, 1):
            x_hop(1, h, hop)

    wait_bytes(ybuf, out_sem)
    chunks = 4 * hz - 2
    for side in (0, 1):
        wait_bytes(w0.at[pl.ds(0, 2), pl.ds(0, chunks)], z_send.at[side])
        for layer in range(LAYERS):
            wait_bytes(att.at[0, pl.ds(0, 2 * hx - 1), pl.ds(0, 2)], att_send.at[layer, side])
            wait_bytes(xbuf.at[pl.ds(0, 2 * hx - 1), 0], x_send.at[layer, side])
    for layer in range(LAYERS):
        wait_bytes(w0.at[pl.ds(0, 2)], part_send.at[layer])
        wait_bytes(kv.at[layer, :, pl.ds(0, 2 * toks)], halo_send.at[layer])
    wait_bytes(wt.at[:, pl.ds(0, nx - 1)], a2a_send)


def reorder_kernel(nx, y, o):
    part = LANES // nx
    tiles = [y[x].reshape(-1, LANES).astype(F32) for x in range(nx)]
    group = lax.broadcasted_iota(jnp.int32, tiles[0].shape, 1) // part
    bit = 1
    while bit < nx:
        low = (group & bit) == 0
        for x in range(nx):
            if x & bit == 0:
                a, b = tiles[x], tiles[x | bit]
                tiles[x] = jnp.where(low, a, pltpu.roll(b, bit * part, 1))
                tiles[x | bit] = jnp.where(low, pltpu.roll(a, LANES - bit * part, 1), b)
        bit *= 2
    for x in range(nx):
        o[:, x * LANES : (x + 1) * LANES] = tiles[x].astype(BF16)


def on_device(tokens, norm_gain, w_query, w_key, w_value, w_out, offset_bias):
    nsp, nx = lax.axis_size("sp"), lax.axis_size("tp")
    nz = nsp // 2
    hz, hx = nz // 2, nx // 2
    toks, depth = tokens.shape
    part = LANES // nx
    piece_w = depth // nx
    wide = 2 * HD
    rows = toks // GRID_W
    half = toks // 2

    def split(w):
        return w.reshape(LAYERS, nx, part, wide)

    gain0 = norm_gain[0].reshape(1, depth)
    gain1 = norm_gain[1].astype(F32).reshape(nsp, nx, part).swapaxes(0, 1).reshape(nx, 1, piece_w)
    table = jnp.pad(offset_bias, ((0, 0), (0, 0), (0, 2), (0, LANES - 2 * KC + 1)))
    lines = jnp.roll(table[:, :, : 2 * KR], 1 - KC, axis=3)
    lines = lines + jnp.roll(table[:, :, 1 : 2 * KR + 1], GRID_W + 1 - KC, axis=3)

    vmem = pl.BlockSpec(memory_space=pltpu.VMEM)
    dma = pltpu.SemaphoreType.DMA
    y = pl.pallas_call(
        functools.partial(layers_kernel, nsp, nx),
        out_shape=jax.ShapeDtypeStruct((nx, 2, half, piece_w), BF16),
        in_specs=[vmem] * 8,
        out_specs=pl.BlockSpec(memory_space=pl.ANY),
        scratch_shapes=[
            pltpu.VMEM((3, nsp, nx, part, wide), BF16),
            pltpu.VMEM((3, nx, nsp, part, wide), BF16),
            pltpu.VMEM((LAYERS, nsp, part, nx * wide), BF16),
            pltpu.VMEM((LAYERS, nx, part, wide), BF16),
            pltpu.VMEM((toks, depth), BF16),
            pltpu.VMEM((toks, 3 * wide), F32),
            pltpu.VMEM((toks, piece_w), BF16),
            pltpu.VMEM((toks, wide), BF16),
            pltpu.VMEM((LAYERS, 2, 3 * toks, wide), BF16),
            pltpu.VMEM((LAYERS, nx, rows, GRID_W, wide), BF16),
            pltpu.VMEM((nx, 2, half, piece_w), BF16),
            pltpu.VMEM((nx, 2, half, piece_w), BF16),
            pltpu.VMEM((toks, LANES), F32),
            dma((LAYERS, 4, 2 * hz)),
            dma((hz + 4,)),
            dma((LAYERS, 2, 2)),
            dma((LAYERS, rows, 2 * hx)),
            dma((LAYERS, 2, 2 * hx)),
            dma((LAYERS,)),
            dma((2,)),
            dma((LAYERS,)),
            dma((LAYERS,)),
            dma((LAYERS, 2)),
            dma((LAYERS, 2)),
            dma(()),
            dma(()),
        ],
        compiler_params=pltpu.CompilerParams(
            collective_id=0, has_side_effects=True, vmem_limit_bytes=60 * 1024 * 1024
        ),
    )(tokens, gain0, gain1, split(w_query), split(w_key), split(w_value), w_out, lines)
    return pl.pallas_call(
        functools.partial(reorder_kernel, nx),
        grid=(piece_w // LANES,),
        out_shape=jax.ShapeDtypeStruct((toks, depth), BF16),
        in_specs=[pl.BlockSpec((nx, 2, half, LANES), lambda g: (0, 0, 0, g))],
        out_specs=pl.BlockSpec((toks, nx * LANES), lambda g: (0, g)),
    )(y)


def solution(mesh):
    return jax.shard_map(
        on_device,
        mesh=mesh,
        in_specs=(
            P(("grp", "sp"), None),
            P(),
            P(None, "sp", "tp"),
            P(None, "sp", "tp"),
            P(None, "sp", "tp"),
            P(None, "tp", "sp"),
            P(None, "tp", None, None),
        ),
        out_specs=P(("grp", "sp"), None),
        check_vma=False,
    )
```

time: 440 us -> 219 us (0.50)
  waiting for transfers between devices: 345 us -> 0 us
  Pallas kernels: 0 us -> 216 us
  local copies, waits for them, and re-layouts: 35.7 us -> 1.68 us
  matrix products: 25.7 us -> 0 us
  between operations: 13.6 us -> 0.04 us
  other arithmetic: 12.2 us -> 1.47 us
  starting transfers between devices: 6.58 us -> 0 us
    all_gather x3 -> x0, waiting for transfers between devices: 243 us -> none  [the longest x1 155 us: turned_gather(): result, at, outs = (lax.all_gather(both, axis, axis=0, tiled=True), 0, [])]
    pallas_call x0 -> x2, Pallas kernels: none -> 216 us  [the longest x1 211 us: on_device(): pl.pallas_call(functools.partial(layers_kernel, nsp, nx), out_shape=jax.S...]
    reduce_scatter x2 -> x0, waiting for transfers between devices: 101 us -> none  [on_device(): lax.psum_scatter(term_rows(jnp.int32(0), lax.axis_size('tp') * share_rows...]
    dot_general x16 -> x0, matrix products: 25.7 us -> none  [the longest x2 5.98 us: on_device(): jnp.dot(normed, every_query[layer_index], preferred_element_type=jnp.floa...]
    unnamed x36 -> x1, local copies, waits for them, and re-layouts: 16.1 us -> 0.76 us
    slice x1 -> x3, local copies, waits for them, and re-layouts: 10.2 us -> 0.09 us  [the longest x2 0.08 us: on_device(): lines = jnp.roll(table[:, :, :2 * KR], 1 - KC, axis=3)]
    ppermute x4 -> x0, starting transfers between devices: 6.14 us -> none  [the longest x2 3.52 us: with_halo(): lax.ppermute(lax.slice_in_dim(block, block.shape[dim] - width, None, axis...]
    concatenate x6 -> x0, other arithmetic: 4.68 us -> none  [the longest x2 2.31 us: with_halo(): block = jnp.concatenate([low, block, high], axis=dim)]
  transfers between devices with their start and end apart: 9 -> 0, of which waited for: 6 -> 0; matrix products, arithmetic and copies ran while one was open for 5% -> 0% of each run, Pallas kernels for 0% -> 0%
where the time goes in v1:
time: 219 us
  Pallas kernels  216 us (99%)
    pallas_call x1, Pallas kernels, on_device(): pl.pallas_call(functools.partial(layers_kernel, nsp, nx), out_shape=jax.S...  211 us
    pallas_call x1, Pallas kernels, on_device(): pl.pallas_call(functools.partial(reorder_kernel, nx), grid=(piece_w // LA...  4.75 us

profile of v1, /device:TPU:80, one launch (start us, length us, event | category | flops | bytes accessed | tf_op | source)
XLA Modules:
  0.0 218.7 jit_solution(6949947709565236949)
XLA Ops:
  0.0 0.8 convert_reduce_fusion
  0.8 0.8 copy.11
  1.6 0.1 pad_slice_fusion.2
  1.6 0.7 maximum_add_fusion.bias
  2.3 0.1 reshape.27
  2.5 0.7 reshape.28.gain1
  3.2 210.8 %shard_map.73.y = bf16[8,2,128,512]{3,2,1,0:T(8,128)(2,1)} custom-call(bf16[256,4096]{1,0:T(8,128)(2,1)} %tok.1, bf16[1,4096]{1,0:T(2,128)(2,1)} %bitcast.9, f32[8,1,512]{2,1,0:T(1,128)} %reshape.28.gain1, bf16[2,8,16,256]{3,2,1,0:T(8,128)(2,1)} %bitcast.6, bf16[2,8,16,256]{3,2,1,0:T(8,128)(2,1)} %bitcast.7, bf16[2,8,16,256]{3,2,1,0:T(8,128)(2,1)} %bitcast.8, ...), custom_call_target="tpu_custom_call" | custom-call | tf_op jit(solution)/shard_map/pallas_call | solution.py:467
  214.0 4.8 %shard_map.74 = bf16[256,4096]{1,0:T(8,128)(2,1)} custom-call(bf16[8,2,128,512]{3,2,1,0:T(8,128)(2,1)} %shard_map.73.y), custom_call_target="tpu_custom_call" | custom-call | tf_op jit(solution)/shard_map/pallas_call | solution.py:504
  (3 shorter events, 0.0 us)

commit v2 on v1

--- a/solution.py
+++ b/solution.py
@@ -44,18 +44,35 @@
     ).start()
 
 
+def exchange(tiles):
+    tiles, n = list(tiles), len(tiles)
+    part = LANES // n
+    group = lax.broadcasted_iota(jnp.int32, tiles[0].shape, 1) // part
+    bit = 1
+    while bit < n:
+        low = (group & bit) == 0
+        for x in range(n):
+            if x & bit == 0:
+                a, b = tiles[x], tiles[x | bit]
+                tiles[x] = jnp.where(low, a, pltpu.roll(b, bit * part, 1))
+                tiles[x | bit] = jnp.where(low, pltpu.roll(a, LANES - bit * part, 1), b)
+        bit *= 2
+    return tiles
+
+
 def layers_kernel(
     nsp,
     nx,
-    tok,
-    gain0,
-    gain1,
+    tok_hbm,
+    gain,
     wq,
     wk,
     wv,
-    wout,
+    wout_hbm,
     bias,
     out,
+    tok,
+    wout,
     w0,
     w1,
     wo,
@@ -69,6 +86,10 @@
     xbuf,
     ybuf,
     ss,
+    gain1,
+    padded,
+    lines,
+    load_sem,
     ring_recv,
     part_recv,
     halo_recv,
@@ -108,24 +129,38 @@
         {"sp": lax.rem(me_s + 1, nsp)},
     )
 
+    mats = (wk, wv, wq)
+    kinds = (0, 1, 2)
+    OUTS = (3, 4)
+    HALVES = (5, 6, 7, 8)
+    parity = (0, 1, 0, 1, 1, 0, 1, 0, 1)
+
+    loads = [pltpu.make_async_copy(mats[k].at[0], w0.at[k, me_s], load_sem.at[k]) for k in kinds]
+    loads += [
+        pltpu.make_async_copy(mats[k].at[1], w1.at[k, :, me_s], load_sem.at[3 + k]) for k in kinds
+    ]
+    loads.append(pltpu.make_async_copy(wout_hbm, wout, load_sem.at[6]))
+    loads.append(pltpu.make_async_copy(tok_hbm, tok, load_sem.at[7]))
+    for load in loads:
+        load.start()
+
     barrier = pltpu.get_barrier_semaphore()
     peers = [*z_dev, *halo_dev] + [{"tp": ring_x(d)} for d in range(1, nx)]
     for peer in peers:
         pl.semaphore_signal(barrier, inc=1, device_id=peer, device_id_type=MESH)
     pl.semaphore_wait(barrier, len(peers))
 
-    mats = (wk, wv, wq)
-    kinds = (0, 1, 2)
-    OUT = 3
-    parity = (0, 1, 0, 1)
-
     def chunk(layer, kind, s):
-        if kind == OUT:
-            return wo.at[layer, s]
+        if kind in OUTS:
+            lanes = nx * wide // 2
+            return wo.at[layer, s, :, pl.ds((kind - OUTS[0]) * lanes, lanes)]
+        if kind in HALVES:
+            which, part_of = divmod(kind - HALVES[0], 2)
+            return w1.at[1 + which, pl.ds(part_of * hx, hx), s]
         return w0.at[kind, s] if layer == 0 else w1.at[kind, :, s]
 
     def part_sem(layer, kind, hop):
-        if kind == OUT:
+        if kind in OUTS:
             return part_recv.at[hz + 1 + layer]
         return part_recv.at[hop] if layer == 0 else part_recv.at[hz + 3]
 
@@ -134,11 +169,10 @@
 
     def ring_start(layer, kind):
         dst = chunk(layer, kind, me_s)
-        src = dst if kind == OUT else mats[kind].at[layer]
         for side in (0, 1):
             if reach(nz, parity[kind])[side] >= 1:
-                send(src, dst, z_send.at[side], ring_slot(layer, kind, side, 1), z_dev[side])
-        send(src, dst, part_send.at[layer], part_sem(layer, kind, 0), partner)
+                send(dst, dst, z_send.at[side], ring_slot(layer, kind, side, 1), z_dev[side])
+        send(dst, dst, part_send.at[layer], part_sem(layer, kind, 0), partner)
 
     def ring_hop(layer, kind, hop):
         for side in (0, 1):
@@ -158,15 +192,28 @@
                 pl.when(hop < last)(onward)
             send(src, src, part_send.at[layer], part_sem(layer, kind, hop), partner)
 
-    pending = []
-
-    def service(count):
-        for _ in range(min(count, len(pending))):
-            ring_hop(*pending.pop(0))
+    def hops(*groups):
+        return [(ring_hop, layer, kind, hop) for layer, kind, hop in groups if 1 <= hop <= hz]
+
+    first = [hops((0, 3, h), (0, 4, h), (1, 0, h)) for h in range(1, hz + 1)]
+    lag = max(hz // 2, 1)
+    second = [
+        hops(*[(1, kind, h) for kind in HALVES], (1, 3, h - lag), (1, 4, h - lag))
+        for h in range(1, hz + lag + 1)
+    ]
+    second[lag - 1] += [(ring_start, 1, kind) for kind in OUTS]
+    first[max(len(first) - 3, 0)] += [(ring_start, 1, kind) for kind in HALVES]
+
+    def service(group, count):
+        for _ in range(min(count, len(group))):
+            for step, *what in group.pop(0):
+                step(*what)
 
     for kind in kinds:
+        loads[kind].wait()
         ring_start(0, kind)
 
+    loads[6].wait()
     eye = (
         lax.broadcasted_iota(jnp.int32, (LANES, LANES), 0)
         == lax.broadcasted_iota(jnp.int32, (LANES, LANES), 1)
@@ -186,23 +233,41 @@
                 {"tp": to},
             )
         wo[layer, me_s, :, own_lanes] = wt[layer, me_x]
-    for kind in kinds:
-        w0[kind, me_s] = mats[kind][0]
-        w1[kind, :, me_s] = mats[kind][1]
-
+    loads[7].wait()
     block = 32
 
     def norm_rows(i, carry):
         at = pl.ds(pl.multiple_of(i * block, block), block)
         x = tok[at, :].astype(F32)
         scaled = x * lax.rsqrt(jnp.mean(x * x, axis=-1, keepdims=True) + norm_eps)
-        xn[at, :] = (scaled * gain0[...].astype(F32)).astype(BF16)
+        xn[at, :] = (scaled * gain[0:1].astype(F32)).astype(BF16)
         return carry
 
     lax.fori_loop(0, toks // block, norm_rows, 0)
 
-    wait_bytes(wt.at[0, pl.ds(0, nx - 1)], a2a_recv.at[0])
-    ring_start(0, OUT)
+    for x, tile in enumerate(
+        exchange(
+            [
+                jnp.concatenate(
+                    [
+                        gain[1:2, (g * nx + t) * LANES : (g * nx + t + 1) * LANES].astype(F32)
+                        for g in range(piece_w // LANES)
+                    ],
+                    axis=0,
+                )
+                for t in range(nx)
+            ]
+        )
+    ):
+        for g in range(piece_w // LANES):
+            gain1[x, :, g * LANES : (g + 1) * LANES] = tile[g : g + 1]
+    padded[...] = jnp.zeros_like(padded)
+    padded[:, : 2 * KR - 1, :, : 2 * KC - 1] = bias[...]
+    for layer in range(LAYERS):
+        for head in (0, 1):
+            here = pltpu.roll(padded[layer, : 2 * KR, head, :], LANES + 1 - KC, 1)
+            after = pltpu.roll(padded[layer, 1 : 2 * KR + 1, head, :], GRID_W + 1 - KC, 1)
+            lines[layer, head] = here + after
 
     def qkv_block(z, kind):
         x = xn[:, pl.ds(pl.multiple_of(z * 2 * LANES, 2 * LANES), 2 * LANES)]
@@ -223,7 +288,7 @@
             )
 
     def ring_step(hop, carry):
-        for kind in (*kinds, OUT):
+        for kind in kinds:
             ring_hop(0, kind, hop)
 
         @pl.when(hop > 1)
@@ -247,8 +312,6 @@
         ring_hop(0, kind, hz)
     if hz > 1:
         two_sides(hz - 1)
-    for kind in kinds:
-        ring_start(1, kind)
     wait_bytes(w0.at[0, pl.ds(0, 3)], part_recv.at[hz])
     far = lax.rem(me_z + hz, nz)
 
@@ -264,8 +327,13 @@
 
     for kind in kinds:
         store_kind(0, kind, acc[:, kind * wide : (kind + 1) * wide] + qkv_block(far, kind))
-    ring_hop(0, OUT, hz)
-    pending += [(1, kind, hop) for hop in range(1, hz + 1) for kind in kinds]
+    for layer in range(LAYERS):
+        wait_bytes(wt.at[layer, pl.ds(0, nx - 1)], a2a_recv.at[layer])
+    for kind in kinds:
+        loads[3 + kind].wait()
+    for kind in OUTS:
+        ring_start(0, kind)
+    ring_start(1, 0)
 
     q_col = lax.broadcasted_iota(jnp.int32, (GRID_W, KR * GRID_W), 0)
     k_col = lax.broadcasted_iota(jnp.int32, (GRID_W, KR * GRID_W), 1) % GRID_W
@@ -273,24 +341,29 @@
     inside = (k_col >= first_col) & (k_col < first_col + KC)
     grid_rows = rows * nsp
 
-    def attend(layer, i, head):
-        row = me_s * rows + i
-        start = jnp.clip(row - KR // 2, 0, grid_rows - KR) - (me_s * rows - rows)
-        keys_at = pl.ds(pl.multiple_of(start * GRID_W, GRID_W), KR * GRID_W)
+    def span(i):
+        start = jnp.clip(me_s * rows + i - KR // 2, 0, grid_rows - KR) - (me_s * rows - rows)
+        return start, pl.ds(pl.multiple_of(start * GRID_W, GRID_W), KR * GRID_W)
+
+    def weigh(layer, i, head):
+        start, keys_at = span(i)
         lanes = slice(head * HD, (head + 1) * HD)
         q = qbuf[i * GRID_W : (i + 1) * GRID_W, lanes]
         scores = nt_dot(q, kv[layer, 0, keys_at, lanes]) * (HD**-0.5)
         offset = start - rows - i + KR - 1
         pairs = []
         for p in range(KR // 2):
-            line = bias[layer, head, pl.ds(offset + 2 * p, 1), :]
+            line = lines[layer, head, pl.ds(offset + 2 * p, 1), :]
             spread = jnp.broadcast_to(line, (GRID_W, LANES))
             pairs.append(pltpu.roll(spread, 0, 1, stride=1, stride_axis=0))
         scores = scores + jnp.concatenate(pairs, axis=1)
         scores = jnp.where(inside, scores, -jnp.inf)
         e = jnp.exp(scores - jnp.max(scores, axis=-1, keepdims=True))
-        weights = (e / jnp.sum(e, axis=-1, keepdims=True)).astype(BF16)
-        values = kv[layer, 1, keys_at, lanes]
+        return (e / jnp.sum(e, axis=-1, keepdims=True)).astype(BF16)
+
+    def mix(layer, i, head, weights):
+        lanes = slice(head * HD, (head + 1) * HD)
+        values = kv[layer, 1, span(i)[1], lanes]
         mixed = jnp.dot(weights, values, preferred_element_type=F32)
         att[layer, me_x, i, :, lanes] = mixed.astype(BF16)
 
@@ -306,22 +379,27 @@
                 slot = att_recv.at[layer, i, side * hx + hop]
                 send(src, src, att_send.at[layer, side], slot, x_dev[side])
 
-    def attention(layer):
-        for kind in (0, 1):
-            for side in (0, 1):
-                dst = kv.at[layer, kind, pl.ds(2 * toks if side == 0 else 0, toks)]
-                wait_bytes(dst, halo_recv.at[layer, kind, side])
-        for i in range(rows):
-            for head in (0, 1):
-                attend(layer, i, head)
+    def halo_wait(layer, kind):
+        for side in (0, 1):
+            dst = kv.at[layer, kind, pl.ds(2 * toks if side == 0 else 0, toks)]
+            wait_bytes(dst, halo_recv.at[layer, kind, side])
+
+    def attention(layer, group, counts):
+        halo_wait(layer, 0)
+        for i in range(0, rows, 2):
+            weights = [weigh(layer, i + n // 2, n % 2) for n in range(4)]
+            if i == 0:
+                halo_wait(layer, 1)
+            for n in range(4):
+                mix(layer, i + n // 2, n % 2, weights[n])
             att_hop(layer, i, 0)
-            if layer == 0:
-                service(1)
+            att_hop(layer, i + 1, 0)
+            service(group, counts[i // 2])
         for hop in range(1, hx + 1):
             for i in range(rows):
                 att_hop(layer, i, hop)
-            if layer == 0:
-                service(2)
+            service(group, counts[1 + hop] if 1 + hop < len(counts) else 1)
+        service(group, len(group))
 
     def x_hop(layer, h, hop):
         buf = xbuf if layer == 0 else ybuf
@@ -353,60 +431,48 @@
             buf[me_x, h] = (own.astype(F32) + total).astype(BF16)
             x_hop(layer, h, 0)
 
-    attention(0)
+    attention(0, first, (1, 1, 1, 2, 2, 1))
     project(0)
 
-    acc[...] = jnp.zeros_like(acc)
     ss[...] = jnp.zeros_like(ss)
 
-    def qkv_piece(owner, h):
-        at = slice(h * half, (h + 1) * half)
-        x = xbuf[owner, h].astype(F32)
-        squares = x * x
-        partial = ss[at]
-        for g in range(piece_w // LANES):
-            partial = partial + squares[:, g * LANES : (g + 1) * LANES]
-        ss[at] = partial
-        xg = (x * gain1[owner]).astype(BF16)
-        for kind in kinds:
-            w = w1[kind, owner].reshape(piece_w, wide)
-            lanes = slice(kind * wide, (kind + 1) * wide)
-            acc[at, lanes] += jnp.dot(xg, w, preferred_element_type=F32)
-
-    def owners(hop):
-        if hop == 0 or hop == hx:
-            return [ring_x(hop)]
-        return [ring_x(-hop), ring_x(hop)]
-
-    early = hx // 2
-    share = -(-len(pending) // max(2 * early, 1))
-    for hop in range(1, early + 1):
+    def take_piece(owner, h):
+        def some_rows(i, carry):
+            at = pl.ds(pl.multiple_of(i * block, block), block)
+            to = pl.ds(pl.multiple_of(h * half + i * block, block), block)
+            x = xbuf[owner, h, at].astype(F32)
+            squares = x * x
+            total = ss[to]
+            for g in range(piece_w // LANES):
+                total = total + squares[:, g * LANES : (g + 1) * LANES]
+            ss[to] = total
+            lanes = pl.ds(pl.multiple_of(owner * piece_w, piece_w), piece_w)
+            xn[to, lanes] = (x * gain1[owner]).astype(BF16)
+            return carry
+
+        lax.fori_loop(0, half // block, some_rows, 0)
+
+    share = -(-hz // hx)
+    for h in (0, 1):
+        take_piece(me_x, h)
+    for hop in range(1, hx + 1):
         for h in (0, 1):
             x_hop(0, h, hop)
-            service(share)
-    service(len(pending))
-    wait_bytes(wt.at[1, pl.ds(0, nx - 1)], a2a_recv.at[1])
-    ring_start(1, OUT)
-    pending += [(1, OUT, hop) for hop in range(1, hz + 1)]
+            if h == 1:
+                service(second, share)
+            for owner in {0: [ring_x(-hop)], 1: [ring_x(hop)]}[h] if hop == hx else [
+                ring_x(-hop),
+                ring_x(hop),
+            ]:
+                take_piece(owner, h)
+    service(second, len(second) - lag)
     wait_bytes(w0.at[:, pl.ds(0, nz)], part_recv.at[hz + 3])
-    for hop in range(0, early + 1):
-        for owner in owners(hop):
-            for h in (0, 1):
-                qkv_piece(owner, h)
-        service(1)
-    for hop in range(early + 1, hx + 1):
-        for h in (0, 1):
-            x_hop(0, h, hop)
-        service(1)
-        for owner in owners(hop):
-            for h in (0, 1):
-                qkv_piece(owner, h)
     mean = jnp.sum(ss[...], axis=-1, keepdims=True) * (1.0 / depth)
     scale = lax.rsqrt(mean + norm_eps)
     for kind in kinds:
-        store_kind(1, kind, acc[:, kind * wide : (kind + 1) * wide] * scale)
-    service(len(pending))
-    attention(1)
+        w = w1[kind].reshape(depth, wide)
+        store_kind(1, kind, jnp.dot(xn[...], w, preferred_element_type=F32) * scale)
+    attention(1, second, (1, 1, 1, 1, 1, 1))
     project(1)
     for hop in range(1, hx + 1):
         for h in (0, 1):
@@ -426,20 +492,19 @@
 
 
 def reorder_kernel(nx, y, o):
-    part = LANES // nx
-    tiles = [y[x].reshape(-1, LANES).astype(F32) for x in range(nx)]
-    group = lax.broadcasted_iota(jnp.int32, tiles[0].shape, 1) // part
-    bit = 1
-    while bit < nx:
-        low = (group & bit) == 0
-        for x in range(nx):
-            if x & bit == 0:
-                a, b = tiles[x], tiles[x | bit]
-                tiles[x] = jnp.where(low, a, pltpu.roll(b, bit * part, 1))
-                tiles[x | bit] = jnp.where(low, pltpu.roll(a, LANES - bit * part, 1), b)
-        bit *= 2
-    for x in range(nx):
-        o[:, x * LANES : (x + 1) * LANES] = tiles[x].astype(BF16)
+    half = y.shape[2]
+    block = 32
+
+    def some_rows(i, carry):
+        at = pl.ds(pl.multiple_of(i * block, block), block)
+        for h in (0, 1):
+            to = pl.ds(pl.multiple_of(h * half + i * block, block), block)
+            tiles = exchange([y[x, h, at, :].astype(F32) for x in range(nx)])
+            for x in range(nx):
+                o[to, x * LANES : (x + 1) * LANES] = tiles[x].astype(BF16)
+        return carry
+
+    lax.fori_loop(0, half // block, some_rows, 0)
 
 
 def on_device(tokens, norm_gain, w_query, w_key, w_value, w_out, offset_bias):
@@ -456,20 +521,17 @@
     def split(w):
         return w.reshape(LAYERS, nx, part, wide)
 
-    gain0 = norm_gain[0].reshape(1, depth)
-    gain1 = norm_gain[1].astype(F32).reshape(nsp, nx, part).swapaxes(0, 1).reshape(nx, 1, piece_w)
-    table = jnp.pad(offset_bias, ((0, 0), (0, 0), (0, 2), (0, LANES - 2 * KC + 1)))
-    lines = jnp.roll(table[:, :, : 2 * KR], 1 - KC, axis=3)
-    lines = lines + jnp.roll(table[:, :, 1 : 2 * KR + 1], GRID_W + 1 - KC, axis=3)
-
     vmem = pl.BlockSpec(memory_space=pltpu.VMEM)
+    hbm = pl.BlockSpec(memory_space=pl.ANY)
     dma = pltpu.SemaphoreType.DMA
     y = pl.pallas_call(
         functools.partial(layers_kernel, nsp, nx),
         out_shape=jax.ShapeDtypeStruct((nx, 2, half, piece_w), BF16),
-        in_specs=[vmem] * 8,
-        out_specs=pl.BlockSpec(memory_space=pl.ANY),
+        in_specs=[hbm, vmem, hbm, hbm, hbm, hbm, vmem],
+        out_specs=hbm,
         scratch_shapes=[
+            pltpu.VMEM((toks, depth), BF16),
+            pltpu.VMEM((LAYERS, wide, LANES), BF16),
             pltpu.VMEM((3, nsp, nx, part, wide), BF16),
             pltpu.VMEM((3, nx, nsp, part, wide), BF16),
             pltpu.VMEM((LAYERS, nsp, part, nx * wide), BF16),
@@ -483,7 +545,11 @@
             pltpu.VMEM((nx, 2, half, piece_w), BF16),
             pltpu.VMEM((nx, 2, half, piece_w), BF16),
             pltpu.VMEM((toks, LANES), F32),
-            dma((LAYERS, 4, 2 * hz)),
+            pltpu.VMEM((nx, 1, piece_w), F32),
+            pltpu.VMEM((LAYERS, 2 * KR + 1, 2, LANES), F32),
+            pltpu.VMEM((LAYERS, 2, 2 * KR, LANES), F32),
+            dma((8,)),
+            dma((LAYERS, 9, 2 * hz)),
             dma((hz + 4,)),
             dma((LAYERS, 2, 2)),
             dma((LAYERS, rows, 2 * hx)),
@@ -500,7 +566,15 @@
         compiler_params=pltpu.CompilerParams(
             collective_id=0, has_side_effects=True, vmem_limit_bytes=60 * 1024 * 1024
         ),
-    )(tokens, gain0, gain1, split(w_query), split(w_key), split(w_value), w_out, lines)
+    )(
+        tokens,
+        norm_gain,
+        split(w_query),
+        split(w_key),
+        split(w_value),
+        w_out,
+        offset_bias.swapaxes(1, 2),
+    )
     return pl.pallas_call(
         functools.partial(reorder_kernel, nx),
         grid=(piece_w // LANES,),

time: 219 us -> 215 us (0.982)
    pallas_call x1, Pallas kernels: 211 us -> 208 us  [on_device(): pl.pallas_call(functools.partial(layers_kernel, nsp, nx), out_shape=jax.S...]
where the time goes in v2:
time: 215 us; the launch traced here: 214 us
  Pallas kernels  214 us (100%)
    pallas_call x1, Pallas kernels, on_device(): pl.pallas_call(functools.partial(layers_kernel, nsp, nx), out_shape=jax.S...  208 us
    pallas_call x1, Pallas kernels, on_device(): pl.pallas_call(functools.partial(reorder_kernel, nx), grid=(piece_w // LA...  6.25 us

profile of v2, /device:TPU:80, one launch (start us, length us, event | category | flops | bytes accessed | tf_op | source)
XLA Modules:
  0.0 214.3 jit_solution(3398096421932281600)
XLA Ops:
  0.0 208.0 %shard_map.73.y = bf16[8,2,128,512]{3,2,1,0:T(8,128)(2,1)} custom-call(bf16[256,4096]{1,0:T(8,128)(2,1)} %tok_hbm.1, bf16[2,4096]{1,0:T(2,128)(2,1)} %gain.1, bf16[2,8,16,256]{3,2,1,0:T(8,128)(2,1)} %bitcast.4, bf16[2,8,16,256]{3,2,1,0:T(8,128)(2,1)} %bitcast.5, bf16[2,8,16,256]{3,2,1,0:T(8,128)(2,1)} %bitcast.6, bf16[2,256,128]{2,1,0:T(8,128)(2,1)} %wout_hbm.1, ...), custom_call_target="tpu_custom_call" | custom-call | tf_op jit(solution)/shard_map/pallas_call | solution.py:527
  208.0 6.3 %shard_map.74 = bf16[256,4096]{1,0:T(8,128)(2,1)} custom-call(bf16[8,2,128,512]{3,2,1,0:T(8,128)(2,1)} %shard_map.73.y), custom_call_target="tpu_custom_call" | custom-call | tf_op jit(solution)/shard_map/pallas_call | solution.py:578

commit v3 on v2

--- a/solution.py
+++ b/solution.py
@@ -131,9 +131,9 @@
 
     mats = (wk, wv, wq)
     kinds = (0, 1, 2)
-    OUTS = (3, 4)
-    HALVES = (5, 6, 7, 8)
-    parity = (0, 1, 0, 1, 1, 0, 1, 0, 1)
+    OUT = 3
+    parity = (0, 1, 0, 1)
+    lag = max(hz // 2, 1)
 
     loads = [pltpu.make_async_copy(mats[k].at[0], w0.at[k, me_s], load_sem.at[k]) for k in kinds]
     loads += [
@@ -151,18 +151,18 @@
     pl.semaphore_wait(barrier, len(peers))
 
     def chunk(layer, kind, s):
-        if kind in OUTS:
-            lanes = nx * wide // 2
-            return wo.at[layer, s, :, pl.ds((kind - OUTS[0]) * lanes, lanes)]
-        if kind in HALVES:
-            which, part_of = divmod(kind - HALVES[0], 2)
-            return w1.at[1 + which, pl.ds(part_of * hx, hx), s]
+        if kind == OUT:
+            return wo.at[layer, s]
         return w0.at[kind, s] if layer == 0 else w1.at[kind, :, s]
 
     def part_sem(layer, kind, hop):
-        if kind in OUTS:
+        if kind == OUT:
             return part_recv.at[hz + 1 + layer]
-        return part_recv.at[hop] if layer == 0 else part_recv.at[hz + 3]
+        if layer == 1:
+            return part_recv.at[hz + 3]
+        if isinstance(hop, int) and hop == hz:
+            return part_recv.at[(hz, hz + 4, hz + 5)[kind]]
+        return part_recv.at[hop]
 
     def ring_slot(layer, kind, side, hop):
         return ring_recv.at[layer, kind, side * hz + hop - 1]
@@ -192,22 +192,22 @@
                 pl.when(hop < last)(onward)
             send(src, src, part_send.at[layer], part_sem(layer, kind, hop), partner)
 
-    def hops(*groups):
-        return [(ring_hop, layer, kind, hop) for layer, kind, hop in groups if 1 <= hop <= hz]
-
-    first = [hops((0, 3, h), (0, 4, h), (1, 0, h)) for h in range(1, hz + 1)]
-    lag = max(hz // 2, 1)
-    second = [
-        hops(*[(1, kind, h) for kind in HALVES], (1, 3, h - lag), (1, 4, h - lag))
-        for h in range(1, hz + lag + 1)
-    ]
-    second[lag - 1] += [(ring_start, 1, kind) for kind in OUTS]
-    first[max(len(first) - 3, 0)] += [(ring_start, 1, kind) for kind in HALVES]
-
-    def service(group, count):
-        for _ in range(min(count, len(group))):
-            for step, *what in group.pop(0):
-                step(*what)
+    offsets = {(0, OUT): lag, (1, 0): hz, (1, 1): hz, (1, 2): hz + lag, (1, OUT): hz + 2 * lag}
+
+    def run_slot(slot):
+        for what, offset in offsets.items():
+            if 1 <= slot - offset <= hz:
+                ring_hop(*what, slot - offset)
+        for what, offset in offsets.items():
+            if slot == offset:
+                ring_start(*what)
+
+    slots = list(range(hz + 1, 2 * hz + 2 * lag + 1))
+
+    def service(count, until=None):
+        for _ in range(min(count, len(slots))):
+            if until is None or slots[0] <= until:
+                run_slot(slots.pop(0))
 
     for kind in kinds:
         loads[kind].wait()
@@ -287,9 +287,11 @@
                 after, kind
             )
 
-    def ring_step(hop, carry):
+    def ring_step(with_out, hop, carry):
         for kind in kinds:
             ring_hop(0, kind, hop)
+        if with_out:
+            ring_hop(0, OUT, hop - lag)
 
         @pl.when(hop > 1)
         def _():
@@ -297,7 +299,13 @@
 
         return carry
 
-    lax.fori_loop(1, hz, ring_step, 0)
+    split_at = min(lag + 1, hz)
+    lax.fori_loop(1, split_at, functools.partial(ring_step, False), 0)
+    for layer in range(LAYERS):
+        wait_bytes(wt.at[layer, pl.ds(0, nx - 1)], a2a_recv.at[layer])
+    if lag < hz:
+        ring_start(0, OUT)
+    lax.fori_loop(split_at, hz, functools.partial(ring_step, True), 0)
 
     group = nx * LANES
     sel_row = lax.broadcasted_iota(jnp.int32, (group, LANES), 0)
@@ -309,10 +317,9 @@
         res[:, g * LANES : (g + 1) * LANES] = picked.astype(BF16)
 
     for kind in kinds:
-        ring_hop(0, kind, hz)
+        loads[3 + kind].wait()
     if hz > 1:
         two_sides(hz - 1)
-    wait_bytes(w0.at[0, pl.ds(0, 3)], part_recv.at[hz])
     far = lax.rem(me_z + hz, nz)
 
     def store_kind(layer, kind, value):
@@ -325,15 +332,17 @@
             dst = kv.at[layer, kind, pl.ds(2 * toks if side == 0 else 0, toks)]
             send(src, dst, halo_send.at[layer], halo_recv.at[layer, kind, side], halo_dev[side])
 
-    for kind in kinds:
+    def finish_kind(kind):
+        wait_bytes(w0.at[0, 0], part_sem(0, kind, hz))
         store_kind(0, kind, acc[:, kind * wide : (kind + 1) * wide] + qkv_block(far, kind))
-    for layer in range(LAYERS):
-        wait_bytes(wt.at[layer, pl.ds(0, nx - 1)], a2a_recv.at[layer])
-    for kind in kinds:
-        loads[3 + kind].wait()
-    for kind in OUTS:
-        ring_start(0, kind)
-    ring_start(1, 0)
+
+    ring_hop(0, 0, hz)
+    ring_hop(0, 1, hz)
+    finish_kind(0)
+    ring_hop(0, 2, hz)
+    finish_kind(1)
+    run_slot(hz)
+    finish_kind(2)
 
     q_col = lax.broadcasted_iota(jnp.int32, (GRID_W, KR * GRID_W), 0)
     k_col = lax.broadcasted_iota(jnp.int32, (GRID_W, KR * GRID_W), 1) % GRID_W
@@ -374,9 +383,9 @@
                 continue
             src = att.at[layer, ring_x(-hop if side == 0 else hop), i]
             if hop > 0:
-                wait_bytes(src, att_recv.at[layer, i, side * hx + hop - 1])
+                wait_bytes(src, att_recv.at[i, side * hx + hop - 1])
             if hop < last:
-                slot = att_recv.at[layer, i, side * hx + hop]
+                slot = att_recv.at[i, side * hx + hop]
                 send(src, src, att_send.at[layer, side], slot, x_dev[side])
 
     def halo_wait(layer, kind):
@@ -384,7 +393,9 @@
             dst = kv.at[layer, kind, pl.ds(2 * toks if side == 0 else 0, toks)]
             wait_bytes(dst, halo_recv.at[layer, kind, side])
 
-    def attention(layer, group, counts):
+    def attention(layer, counts, until):
+        if layer == 0:
+            service(1)
         halo_wait(layer, 0)
         for i in range(0, rows, 2):
             weights = [weigh(layer, i + n // 2, n % 2) for n in range(4)]
@@ -394,12 +405,12 @@
                 mix(layer, i + n // 2, n % 2, weights[n])
             att_hop(layer, i, 0)
             att_hop(layer, i + 1, 0)
-            service(group, counts[i // 2])
+            service(counts[i // 2])
         for hop in range(1, hx + 1):
             for i in range(rows):
                 att_hop(layer, i, hop)
-            service(group, counts[1 + hop] if 1 + hop < len(counts) else 1)
-        service(group, len(group))
+            service(counts[1 + hop] if 1 + hop < len(counts) else 0)
+        service(len(slots), until)
 
     def x_hop(layer, h, hop):
         buf = xbuf if layer == 0 else ybuf
@@ -410,9 +421,9 @@
             owner = ring_x(-hop if side == 0 else hop)
             src = buf.at[owner, h]
             if hop > 0:
-                wait_bytes(src, x_recv.at[layer, h, side * hx + hop - 1])
+                wait_bytes(src, x_recv.at[h, side * hx + hop - 1])
             if hop < last:
-                slot = x_recv.at[layer, h, side * hx + hop]
+                slot = x_recv.at[h, side * hx + hop]
                 send(src, src, x_send.at[layer, side], slot, x_dev[side])
             if layer == 1 and (hop > 0 or side == 0):
                 pltpu.make_async_copy(src, out.at[owner, h], out_sem).start()
@@ -431,7 +442,7 @@
             buf[me_x, h] = (own.astype(F32) + total).astype(BF16)
             x_hop(layer, h, 0)
 
-    attention(0, first, (1, 1, 1, 2, 2, 1))
+    attention(0, (1, 1, 1, 1, 0, 0), hz + lag)
     project(0)
 
     ss[...] = jnp.zeros_like(ss)
@@ -452,27 +463,23 @@
 
         lax.fori_loop(0, half // block, some_rows, 0)
 
-    share = -(-hz // hx)
     for h in (0, 1):
         take_piece(me_x, h)
     for hop in range(1, hx + 1):
         for h in (0, 1):
+            service(1, 2 * hz + lag)
             x_hop(0, h, hop)
-            if h == 1:
-                service(second, share)
-            for owner in {0: [ring_x(-hop)], 1: [ring_x(hop)]}[h] if hop == hx else [
-                ring_x(-hop),
-                ring_x(hop),
-            ]:
+            both = [ring_x(-hop), ring_x(hop)]
+            for owner in both if hop < hx else both[:1]:
                 take_piece(owner, h)
-    service(second, len(second) - lag)
+    service(len(slots), 2 * hz + lag)
     wait_bytes(w0.at[:, pl.ds(0, nz)], part_recv.at[hz + 3])
     mean = jnp.sum(ss[...], axis=-1, keepdims=True) * (1.0 / depth)
     scale = lax.rsqrt(mean + norm_eps)
     for kind in kinds:
         w = w1[kind].reshape(depth, wide)
         store_kind(1, kind, jnp.dot(xn[...], w, preferred_element_type=F32) * scale)
-    attention(1, second, (1, 1, 1, 1, 1, 1))
+    attention(1, (1, 1, 1, 1, 0, 0), 2 * hz + 2 * lag)
     project(1)
     for hop in range(1, hx + 1):
         for h in (0, 1):
@@ -549,11 +556,11 @@
             pltpu.VMEM((LAYERS, 2 * KR + 1, 2, LANES), F32),
             pltpu.VMEM((LAYERS, 2, 2 * KR, LANES), F32),
             dma((8,)),
-            dma((LAYERS, 9, 2 * hz)),
-            dma((hz + 4,)),
+            dma((LAYERS, 4, 2 * hz)),
+            dma((hz + 6,)),
             dma((LAYERS, 2, 2)),
-            dma((LAYERS, rows, 2 * hx)),
-            dma((LAYERS, 2, 2 * hx)),
+            dma((rows, 2 * hx)),
+            dma((2, 2 * hx)),
             dma((LAYERS,)),
             dma((2,)),
             dma((LAYERS,)),

time: 215 us -> 204 us (0.949)
  Pallas kernels: 214 us -> 204 us
    pallas_call x1, Pallas kernels: 208 us -> 197 us  [on_device(): pl.pallas_call(functools.partial(layers_kernel, nsp, nx), out_shape=jax.S...]
where the time goes in v3:
time: 204 us
  Pallas kernels  204 us (100%)
    pallas_call x1, Pallas kernels, on_device(): pl.pallas_call(functools.partial(layers_kernel, nsp, nx), out_shape=jax.S...  197 us
    pallas_call x1, Pallas kernels, on_device(): pl.pallas_call(functools.partial(reorder_kernel, nx), grid=(piece_w // LA...  6.25 us

profile of v3, /device:TPU:80, one launch (start us, length us, event | category | flops | bytes accessed | tf_op | source)
XLA Modules:
  0.0 203.6 jit_solution(11117579615911126152)
XLA Ops:
  0.0 197.3 %shard_map.73.y = bf16[8,2,128,512]{3,2,1,0:T(8,128)(2,1)} custom-call(bf16[256,4096]{1,0:T(8,128)(2,1)} %tok_hbm.1, bf16[2,4096]{1,0:T(2,128)(2,1)} %gain.1, bf16[2,8,16,256]{3,2,1,0:T(8,128)(2,1)} %bitcast.4, bf16[2,8,16,256]{3,2,1,0:T(8,128)(2,1)} %bitcast.5, bf16[2,8,16,256]{3,2,1,0:T(8,128)(2,1)} %bitcast.6, bf16[2,256,128]{2,1,0:T(8,128)(2,1)} %wout_hbm.1, ...), custom_call_target="tpu_custom_call" | custom-call | tf_op jit(solution)/shard_map/pallas_call | solution.py:534
  197.3 6.3 %shard_map.74 = bf16[256,4096]{1,0:T(8,128)(2,1)} custom-call(bf16[8,2,128,512]{3,2,1,0:T(8,128)(2,1)} %shard_map.73.y), custom_call_target="tpu_custom_call" | custom-call | tf_op jit(solution)/shard_map/pallas_call | solution.py:585

commit v4 on v3

--- a/solution.py
+++ b/solution.py
@@ -133,7 +133,8 @@
     kinds = (0, 1, 2)
     OUT = 3
     parity = (0, 1, 0, 1)
-    lag = max(hz // 2, 1)
+    lag = max(hz // 4, 1)
+    out_from = hz + max(3 * hz // 4, 1)
 
     loads = [pltpu.make_async_copy(mats[k].at[0], w0.at[k, me_s], load_sem.at[k]) for k in kinds]
     loads += [
@@ -192,7 +193,7 @@
                 pl.when(hop < last)(onward)
             send(src, src, part_send.at[layer], part_sem(layer, kind, hop), partner)
 
-    offsets = {(0, OUT): lag, (1, 0): hz, (1, 1): hz, (1, 2): hz + lag, (1, OUT): hz + 2 * lag}
+    offsets = {(0, OUT): lag, (1, 0): hz, (1, 1): hz, (1, 2): hz, (1, OUT): out_from}
 
     def run_slot(slot):
         for what, offset in offsets.items():
@@ -202,7 +203,7 @@
             if slot == offset:
                 ring_start(*what)
 
-    slots = list(range(hz + 1, 2 * hz + 2 * lag + 1))
+    slots = list(range(hz + 1, out_from + hz + 1))
 
     def service(count, until=None):
         for _ in range(min(count, len(slots))):
@@ -394,8 +395,6 @@
             wait_bytes(dst, halo_recv.at[layer, kind, side])
 
     def attention(layer, counts, until):
-        if layer == 0:
-            service(1)
         halo_wait(layer, 0)
         for i in range(0, rows, 2):
             weights = [weigh(layer, i + n // 2, n % 2) for n in range(4)]
@@ -442,7 +441,7 @@
             buf[me_x, h] = (own.astype(F32) + total).astype(BF16)
             x_hop(layer, h, 0)
 
-    attention(0, (1, 1, 1, 1, 0, 0), hz + lag)
+    attention(0, (1, 0, 1, 0, 1, 0), hz + lag)
     project(0)
 
     ss[...] = jnp.zeros_like(ss)
@@ -467,19 +466,21 @@
         take_piece(me_x, h)
     for hop in range(1, hx + 1):
         for h in (0, 1):
-            service(1, 2 * hz + lag)
+            if 2 * hop - 2 + h in (0, 1, 3, 5, 6):
+                service(1, 2 * hz)
             x_hop(0, h, hop)
             both = [ring_x(-hop), ring_x(hop)]
             for owner in both if hop < hx else both[:1]:
                 take_piece(owner, h)
-    service(len(slots), 2 * hz + lag)
+    service(len(slots), 2 * hz)
     wait_bytes(w0.at[:, pl.ds(0, nz)], part_recv.at[hz + 3])
     mean = jnp.sum(ss[...], axis=-1, keepdims=True) * (1.0 / depth)
     scale = lax.rsqrt(mean + norm_eps)
     for kind in kinds:
         w = w1[kind].reshape(depth, wide)
         store_kind(1, kind, jnp.dot(xn[...], w, preferred_element_type=F32) * scale)
-    attention(1, (1, 1, 1, 1, 0, 0), 2 * hz + 2 * lag)
+        service(1 if kind < 2 else 0)
+    attention(1, (1, 1, 1, 1, 0, 0), out_from + hz)
     project(1)
     for hop in range(1, hx + 1):
         for h in (0, 1):
@@ -499,19 +500,9 @@
 
 
 def reorder_kernel(nx, y, o):
-    half = y.shape[2]
-    block = 32
-
-    def some_rows(i, carry):
-        at = pl.ds(pl.multiple_of(i * block, block), block)
-        for h in (0, 1):
-            to = pl.ds(pl.multiple_of(h * half + i * block, block), block)
-            tiles = exchange([y[x, h, at, :].astype(F32) for x in range(nx)])
-            for x in range(nx):
-                o[to, x * LANES : (x + 1) * LANES] = tiles[x].astype(BF16)
-        return carry
-
-    lax.fori_loop(0, half // block, some_rows, 0)
+    tiles = exchange([y[x].reshape(-1, LANES).astype(F32) for x in range(nx)])
+    for x in range(nx):
+        o[:, x * LANES : (x + 1) * LANES] = tiles[x].astype(BF16)
 
 
 def on_device(tokens, norm_gain, w_query, w_key, w_value, w_out, offset_bias):

time: 204 us -> 197 us (0.966)
  Pallas kernels: 204 us -> 197 us
    pallas_call x1, Pallas kernels: 197 us -> 192 us  [on_device(): pl.pallas_call(functools.partial(layers_kernel, nsp, nx), out_shape=jax.S...]
where the time goes in v4:
time: 197 us
  Pallas kernels  197 us (100%)
    pallas_call x1, Pallas kernels, on_device(): pl.pallas_call(functools.partial(layers_kernel, nsp, nx), out_shape=jax.S...  192 us
    pallas_call x1, Pallas kernels, on_device(): pl.pallas_call(functools.partial(reorder_kernel, nx), grid=(piece_w // LA...  4.75 us

profile of v4, /device:TPU:80, one launch (start us, length us, event | category | flops | bytes accessed | tf_op | source)
XLA Modules:
  0.0 197.1 jit_solution(12823773207071563400)
XLA Ops:
  0.0 192.4 %shard_map.73.y = bf16[8,2,128,512]{3,2,1,0:T(8,128)(2,1)} custom-call(bf16[256,4096]{1,0:T(8,128)(2,1)} %tok_hbm.1, bf16[2,4096]{1,0:T(2,128)(2,1)} %gain.1, bf16[2,8,16,256]{3,2,1,0:T(8,128)(2,1)} %bitcast.4, bf16[2,8,16,256]{3,2,1,0:T(8,128)(2,1)} %bitcast.5, bf16[2,8,16,256]{3,2,1,0:T(8,128)(2,1)} %bitcast.6, bf16[2,256,128]{2,1,0:T(8,128)(2,1)} %wout_hbm.1, ...), custom_call_target="tpu_custom_call" | custom-call | tf_op jit(solution)/shard_map/pallas_call | solution.py:525
  192.4 4.8 %shard_map.74 = bf16[256,4096]{1,0:T(8,128)(2,1)} custom-call(bf16[8,2,128,512]{3,2,1,0:T(8,128)(2,1)} %shard_map.73.y), custom_call_target="tpu_custom_call" | custom-call | tf_op jit(solution)/shard_map/pallas_call | solution.py:576

commit v5 on v4

--- a/solution.py
+++ b/solution.py
@@ -132,7 +132,7 @@
     mats = (wk, wv, wq)
     kinds = (0, 1, 2)
     OUT = 3
-    parity = (0, 1, 0, 1)
+    parity = (0, 1, 0, 1, 1)
     lag = max(hz // 4, 1)
     out_from = hz + max(3 * hz // 4, 1)
 
@@ -152,12 +152,13 @@
     pl.semaphore_wait(barrier, len(peers))
 
     def chunk(layer, kind, s):
-        if kind == OUT:
-            return wo.at[layer, s]
+        if kind >= OUT:
+            lanes = nx * wide // (1 + layer)
+            return wo.at[layer, s, :, pl.ds((kind - OUT) * lanes, lanes)]
         return w0.at[kind, s] if layer == 0 else w1.at[kind, :, s]
 
     def part_sem(layer, kind, hop):
-        if kind == OUT:
+        if kind >= OUT:
             return part_recv.at[hz + 1 + layer]
         if layer == 1:
             return part_recv.at[hz + 3]
@@ -166,7 +167,7 @@
         return part_recv.at[hop]
 
     def ring_slot(layer, kind, side, hop):
-        return ring_recv.at[layer, kind, side * hz + hop - 1]
+        return ring_recv.at[4 * layer + kind, side * hz + hop - 1]
 
     def ring_start(layer, kind):
         dst = chunk(layer, kind, me_s)
@@ -193,12 +194,17 @@
                 pl.when(hop < last)(onward)
             send(src, src, part_send.at[layer], part_sem(layer, kind, hop), partner)
 
-    offsets = {(0, OUT): lag, (1, 0): hz, (1, 1): hz, (1, 2): hz, (1, OUT): out_from}
+    offsets = {(0, OUT): lag, (1, 0): hz, (1, 1): hz, (1, 2): hz}
+    offsets |= {(1, OUT): out_from, (1, OUT + 1): out_from}
 
     def run_slot(slot):
         for what, offset in offsets.items():
             if 1 <= slot - offset <= hz:
                 ring_hop(*what, slot - offset)
+        if slot != hz:
+            start_after(slot)
+
+    def start_after(slot):
         for what, offset in offsets.items():
             if slot == offset:
                 ring_start(*what)
@@ -396,6 +402,8 @@
 
     def attention(layer, counts, until):
         halo_wait(layer, 0)
+        if layer == 0:
+            start_after(hz)
         for i in range(0, rows, 2):
             weights = [weigh(layer, i + n // 2, n % 2) for n in range(4)]
             if i == 0:
@@ -441,7 +449,7 @@
             buf[me_x, h] = (own.astype(F32) + total).astype(BF16)
             x_hop(layer, h, 0)
 
-    attention(0, (1, 0, 1, 0, 1, 0), hz + lag)
+    attention(0, (0, 1, 0, 1, 0, 1), hz + lag)
     project(0)
 
     ss[...] = jnp.zeros_like(ss)
@@ -479,8 +487,8 @@
     for kind in kinds:
         w = w1[kind].reshape(depth, wide)
         store_kind(1, kind, jnp.dot(xn[...], w, preferred_element_type=F32) * scale)
-        service(1 if kind < 2 else 0)
-    attention(1, (1, 1, 1, 1, 0, 0), out_from + hz)
+        service(1 if kind == 1 else 0)
+    attention(1, (1, 1, 1, 1, 1, 0), out_from + hz)
     project(1)
     for hop in range(1, hx + 1):
         for h in (0, 1):
@@ -547,7 +555,7 @@
             pltpu.VMEM((LAYERS, 2 * KR + 1, 2, LANES), F32),
             pltpu.VMEM((LAYERS, 2, 2 * KR, LANES), F32),
             dma((8,)),
-            dma((LAYERS, 4, 2 * hz)),
+            dma((9, 2 * hz)),
             dma((hz + 6,)),
             dma((LAYERS, 2, 2)),
             dma((rows, 2 * hx)),

time: 197 us -> 195 us (0.990)
  Pallas kernels: 197 us -> 194 us
    pallas_call x1, Pallas kernels: 192 us -> 190 us  [on_device(): pl.pallas_call(functools.partial(layers_kernel, nsp, nx), out_shape=jax.S...]
where the time goes in v5:
time: 195 us; the launch traced here: 194 us
  Pallas kernels  194 us (99%)
    pallas_call x1, Pallas kernels, on_device(): pl.pallas_call(functools.partial(layers_kernel, nsp, nx), out_shape=jax.S...  190 us
    pallas_call x1, Pallas kernels, on_device(): pl.pallas_call(functools.partial(reorder_kernel, nx), grid=(piece_w // LA...  4.75 us

profile of v5, /device:TPU:80, one launch (start us, length us, event | category | flops | bytes accessed | tf_op | source)
XLA Modules:
  0.0 194.3 jit_solution(12027585415710643699)
XLA Ops:
  0.0 189.5 %shard_map.73.y = bf16[8,2,128,512]{3,2,1,0:T(8,128)(2,1)} custom-call(bf16[256,4096]{1,0:T(8,128)(2,1)} %tok_hbm.1, bf16[2,4096]{1,0:T(2,128)(2,1)} %gain.1, bf16[2,8,16,256]{3,2,1,0:T(8,128)(2,1)} %bitcast.4, bf16[2,8,16,256]{3,2,1,0:T(8,128)(2,1)} %bitcast.5, bf16[2,8,16,256]{3,2,1,0:T(8,128)(2,1)} %bitcast.6, bf16[2,256,128]{2,1,0:T(8,128)(2,1)} %wout_hbm.1, ...), custom_call_target="tpu_custom_call" | custom-call | tf_op jit(solution)/shard_map/pallas_call | solution.py:533
  189.6 4.8 %shard_map.74 = bf16[256,4096]{1,0:T(8,128)(2,1)} custom-call(bf16[8,2,128,512]{3,2,1,0:T(8,128)(2,1)} %shard_map.73.y), custom_call_target="tpu_custom_call" | custom-call | tf_op jit(solution)/shard_map/pallas_call | solution.py:584

commit v6 on v5

--- a/solution.py
+++ b/solution.py
@@ -449,7 +449,7 @@
             buf[me_x, h] = (own.astype(F32) + total).astype(BF16)
             x_hop(layer, h, 0)
 
-    attention(0, (0, 1, 0, 1, 0, 1), hz + lag)
+    attention(0, (0, 0, 1, 0, 1, 0), hz + lag)
     project(0)
 
     ss[...] = jnp.zeros_like(ss)
@@ -474,7 +474,7 @@
         take_piece(me_x, h)
     for hop in range(1, hx + 1):
         for h in (0, 1):
-            if 2 * hop - 2 + h in (0, 1, 3, 5, 6):
+            if 2 * hop - 2 + h in (0, 1, 2, 4, 5, 6):
                 service(1, 2 * hz)
             x_hop(0, h, hop)
             both = [ring_x(-hop), ring_x(hop)]
@@ -488,7 +488,7 @@
         w = w1[kind].reshape(depth, wide)
         store_kind(1, kind, jnp.dot(xn[...], w, preferred_element_type=F32) * scale)
         service(1 if kind == 1 else 0)
-    attention(1, (1, 1, 1, 1, 1, 0), out_from + hz)
+    attention(1, (0, 1, 1, 1, 1, 1), out_from + hz)
     project(1)
     for hop in range(1, hx + 1):
         for h in (0, 1):

time: 195 us -> 195 us (level)
  no operation moved by 1% of the time
where the time goes in v6:
time: 195 us; the launch traced here: 194 us
  Pallas kernels  194 us (99%)
    pallas_call x1, Pallas kernels, on_device(): pl.pallas_call(functools.partial(layers_kernel, nsp, nx), out_shape=jax.S...  189 us
    pallas_call x1, Pallas kernels, on_device(): pl.pallas_call(functools.partial(reorder_kernel, nx), grid=(piece_w // LA...  4.75 us

profile of v6, /device:TPU:80, one launch (start us, length us, event | category | flops | bytes accessed | tf_op | source)
XLA Modules:
  0.0 193.8 jit_solution(15577629537916806408)
XLA Ops:
  0.0 189.0 %shard_map.73.y = bf16[8,2,128,512]{3,2,1,0:T(8,128)(2,1)} custom-call(bf16[256,4096]{1,0:T(8,128)(2,1)} %tok_hbm.1, bf16[2,4096]{1,0:T(2,128)(2,1)} %gain.1, bf16[2,8,16,256]{3,2,1,0:T(8,128)(2,1)} %bitcast.4, bf16[2,8,16,256]{3,2,1,0:T(8,128)(2,1)} %bitcast.5, bf16[2,8,16,256]{3,2,1,0:T(8,128)(2,1)} %bitcast.6, bf16[2,256,128]{2,1,0:T(8,128)(2,1)} %wout_hbm.1, ...), custom_call_target="tpu_custom_call" | custom-call | tf_op jit(solution)/shard_map/pallas_call | solution.py:533
  189.0 4.8 %shard_map.74 = bf16[256,4096]{1,0:T(8,128)(2,1)} custom-call(bf16[8,2,128,512]{3,2,1,0:T(8,128)(2,1)} %shard_map.73.y), custom_call_target="tpu_custom_call" | custom-call | tf_op jit(solution)/shard_map/pallas_call | solution.py:584

commit v7 on v6

--- a/solution.py
+++ b/solution.py
@@ -134,7 +134,7 @@
     OUT = 3
     parity = (0, 1, 0, 1, 1)
     lag = max(hz // 4, 1)
-    out_from = hz + max(3 * hz // 4, 1)
+    out_from = 2 * hz
 
     loads = [pltpu.make_async_copy(mats[k].at[0], w0.at[k, me_s], load_sem.at[k]) for k in kinds]
     loads += [
@@ -488,7 +488,7 @@
         w = w1[kind].reshape(depth, wide)
         store_kind(1, kind, jnp.dot(xn[...], w, preferred_element_type=F32) * scale)
         service(1 if kind == 1 else 0)
-    attention(1, (0, 1, 1, 1, 1, 1), out_from + hz)
+    attention(1, (1, 1, 1, 1, 1, 1), out_from + hz)
     project(1)
     for hop in range(1, hx + 1):
         for h in (0, 1):

time: 195 us -> 199 us (1.021)
  Pallas kernels: 194 us -> 198 us
    pallas_call x1, Pallas kernels: 189 us -> 193 us  [on_device(): pl.pallas_call(functools.partial(layers_kernel, nsp, nx), out_shape=jax.S...]
where the time goes in v7:
time: 199 us; the launch traced here: 198 us
  Pallas kernels  198 us (99%)
    pallas_call x1, Pallas kernels, on_device(): pl.pallas_call(functools.partial(layers_kernel, nsp, nx), out_shape=jax.S...  193 us
    pallas_call x1, Pallas kernels, on_device(): pl.pallas_call(functools.partial(reorder_kernel, nx), grid=(piece_w // LA...  4.75 us

profile of v7, /device:TPU:80, one launch (start us, length us, event | category | flops | bytes accessed | tf_op | source)
XLA Modules:
  0.0 197.7 jit_solution(4122707076807063997)
XLA Ops:
  0.0 192.9 %shard_map.73.y = bf16[8,2,128,512]{3,2,1,0:T(8,128)(2,1)} custom-call(bf16[256,4096]{1,0:T(8,128)(2,1)} %tok_hbm.1, bf16[2,4096]{1,0:T(2,128)(2,1)} %gain.1, bf16[2,8,16,256]{3,2,1,0:T(8,128)(2,1)} %bitcast.4, bf16[2,8,16,256]{3,2,1,0:T(8,128)(2,1)} %bitcast.5, bf16[2,8,16,256]{3,2,1,0:T(8,128)(2,1)} %bitcast.6, bf16[2,256,128]{2,1,0:T(8,128)(2,1)} %wout_hbm.1, ...), custom_call_target="tpu_custom_call" | custom-call | tf_op jit(solution)/shard_map/pallas_call | solution.py:533
  192.9 4.8 %shard_map.74 = bf16[256,4096]{1,0:T(8,128)(2,1)} custom-call(bf16[8,2,128,512]{3,2,1,0:T(8,128)(2,1)} %shard_map.73.y), custom_call_target="tpu_custom_call" | custom-call | tf_op jit(solution)/shard_map/pallas_call | solution.py:584
